TPU v7x, 128 devices: a whole 4x4x4 slice. The times are simulated.
128 devices in a mesh: ep: 128 (over z, y, x, core).
Axes of the slice: x: 4, y: 4, z: 4, core: 2. Of those that a mesh axis runs over, the one named last changes fastest.
Arguments:
- residual_in: bfloat16 [1024, 2048], P('ep'), may hold values from -6 to 6
- gain_mix_pre: float32 [2048], replicated, may hold values from 0.1 to 1.9
- w_query: bfloat16 [2048, 2048], P(None, 'ep'), may hold values from -0.125 to 0.125
- w_key: bfloat16 [2048, 2048], P(None, 'ep'), may hold values from -0.125 to 0.125
- w_value: bfloat16 [2048, 2048], P(None, 'ep'), may hold values from -0.125 to 0.125
- w_outgate: bfloat16 [2048, 2048], P(None, 'ep'), may hold values from -0.125 to 0.125
- w_decay: bfloat16 [2048, 16], replicated, may hold values from -0.125 to 0.125
- w_beta: bfloat16 [2048, 16], replicated, may hold values from -0.125 to 0.125
- decay_scale: float32 [16], replicated, may hold values from 1 to 16
- decay_bias: float32 [16], replicated, may hold values from -5 to -1
- head_gain: float32 [128], replicated, may hold values from 0.1 to 1.9
- w_out: bfloat16 [2048, 2048], replicated, may hold values from -0.125 to 0.125
- gain_mix_post: float32 [2048], replicated, may hold values from 0.1 to 1.9
- state_cache: bfloat16 [1024, 16, 128, 128], P('ep'), may hold values from -2.390625 to 2.390625
- gain_ffn_pre: float32 [2048], replicated, may hold values from 0.1 to 1.9
- routes: int32 [1024, 4], P('ep'), may hold values from 0 to 31, all different within a row; in each aligned block of 8 rows (0 to 7, 8 to 15, ...) at most 2 rows name the same one
- route_logits: float32 [1024, 4], P('ep'), may hold values from -6 to 6
- w_gate: bfloat16 [2048, 65536], P(None, 'ep'), may hold values from -0.375 to 0.375
- w_up: bfloat16 [2048, 65536], P(None, 'ep'), may hold values from -0.375 to 0.375
- w_down: bfloat16 [65536, 2048], P('ep'), may hold values from -0.125 to 0.125
- gain_ffn_post: float32 [2048], replicated, may hold values from 0.1 to 1.9
Outputs:
- result: bfloat16 [1024, 2048], P('ep')
- new_state: bfloat16 [1024, 16, 128, 128], P('ep')
Inputs may be any that keep to these rules, and one draw needn't show every extreme that they name: `routes`: each row names 4 different experts. In the rows of one device (aligned blocks of 8 rows) no expert is named more than 2 times, and in some block one expert is named exactly 2 times.
All inputs are finite; a program needn't handle non-finite values.
Results may differ from a plain program's by a relative error of at most 0.014.
Values may be sent and summed in bfloat16 or wider, within the bound.
No kernel may reach another device: no remote copies, remote signals or barrier semaphores. Data moves between devices by JAX's collectives and lax.ppermute only.
A program may use at most 128 MiB of HBM per device.

v0:
```python
import jax
import jax.numpy as jnp
from jax import lax
from jax.sharding import PartitionSpec as P

H = 16
HD = 128
PIECES = 4
TOPK = 4
EPS = 1e-06
LIMIT = 7.0
ALPHA = 1.702


def rms_scale(values):
    return values * lax.rsqrt(jnp.mean(values * values, axis=-1, keepdims=True) + EPS)


def clamped_unit(gate, upper):
    glu = jnp.minimum(gate, LIMIT)
    linear = jnp.clip(upper, -LIMIT, LIMIT)
    return glu * jax.nn.sigmoid(ALPHA * glu) * (linear + 1.0)


def dispatch_table(routes, experts, capacity):
    count, topk = routes.shape
    hits = (routes[:, :, None] == jnp.arange(experts, dtype=jnp.int32)).astype(jnp.int32)
    flat = hits.reshape(count * topk, experts)
    before = jnp.cumsum(flat, axis=0) - flat
    slots = jnp.sum(before * flat, axis=1).reshape(count, topk)
    target = routes * capacity + slots
    return (target[:, :, None] == jnp.arange(experts * capacity, dtype=jnp.int32)).astype(
        jnp.float32
    )


def delta_step(
    q_raw, k_raw, v_raw, z_raw, decay_in, beta_in, state, decay_scale, decay_bias, head_gain
):
    count = q_raw.shape[0]
    query = jax.nn.silu(q_raw.astype(jnp.float32)).reshape(count, H, HD)
    query = query * lax.rsqrt(jnp.sum(query * query, axis=-1, keepdims=True) + EPS) * HD ** (-0.5)
    keys = jax.nn.silu(k_raw.astype(jnp.float32)).reshape(count, H, HD)
    keys = keys * lax.rsqrt(jnp.sum(keys * keys, axis=-1, keepdims=True) + EPS)
    values = jax.nn.silu(v_raw.astype(jnp.float32)).reshape(count, H, HD)
    decay = -decay_scale * jax.nn.softplus(decay_in + decay_bias)
    beta = jax.nn.sigmoid(beta_in)
    held = state.astype(jnp.float32) * jnp.exp(decay)[:, :, None, None]
    guess = jnp.einsum("rhk,rhkv->rhv", keys, held)
    held = held + jnp.einsum("rhk,rhv->rhkv", keys, beta[:, :, None] * (values - guess))
    output = jnp.einsum("rhk,rhkv->rhv", query, held)
    output = rms_scale(output) * head_gain
    gated = output.reshape(count, H * HD) * jax.nn.silu(z_raw.astype(jnp.float32))
    return (gated.astype(jnp.bfloat16), held.astype(jnp.bfloat16))


def shards(
    residual_in,
    gain_mix_pre,
    w_query,
    w_key,
    w_value,
    w_outgate,
    w_decay,
    w_beta,
    decay_scale,
    decay_bias,
    head_gain,
    w_out,
    gain_mix_post,
    state_cache,
    gain_ffn_pre,
    routes,
    route_logits,
    w_gate,
    w_up,
    w_down,
    gain_ffn_post,
):
    devices = lax.axis_size("ep")
    count, width = residual_in.shape
    x_first = residual_in.astype(jnp.float32)
    normed = (rms_scale(x_first) * gain_mix_pre).astype(jnp.bfloat16)
    stacked = jnp.stack([w_query, w_key, w_value, w_outgate])
    columns = jnp.einsum(
        "td,rdc->trc",
        lax.all_gather(normed, "ep", axis=0, tiled=True),
        stacked,
        preferred_element_type=jnp.float32,
    ).astype(jnp.bfloat16)
    joined = lax.all_to_all(columns, "ep", split_axis=0, concat_axis=2, tiled=True)
    decay_in = jnp.dot(normed, w_decay, preferred_element_type=jnp.float32)
    beta_in = jnp.dot(normed, w_beta, preferred_element_type=jnp.float32)
    mixed, new_state = delta_step(
        joined[:, 0],
        joined[:, 1],
        joined[:, 2],
        joined[:, 3],
        decay_in,
        beta_in,
        state_cache,
        decay_scale,
        decay_bias,
        head_gain,
    )
    branch = jnp.dot(mixed, w_out, preferred_element_type=jnp.float32)
    x_second = x_first + rms_scale(branch) * gain_mix_post
    normed_two = (rms_scale(x_second) * gain_ffn_pre).astype(jnp.bfloat16)
    experts = devices // PIECES
    capacity = max(2, 2 * count * TOPK // experts)
    table = dispatch_table(routes, experts, capacity)
    picks = jnp.sum(table, axis=1).astype(jnp.bfloat16)
    sent = lax.dot_general(
        picks, normed_two, (((0,), (0,)), ((), ())), preferred_element_type=jnp.float32
    ).astype(jnp.bfloat16)
    sent = jnp.broadcast_to(
        sent.reshape(experts, 1, capacity, width), (experts, PIECES, capacity, width)
    ).reshape(devices, capacity, width)
    block = lax.all_to_all(sent, "ep", split_axis=0, concat_axis=0, tiled=True)
    flat = block.reshape(-1, width)
    hidden = clamped_unit(
        jnp.dot(flat, w_gate, preferred_element_type=jnp.float32),
        jnp.dot(flat, w_up, preferred_element_type=jnp.float32),
    ).astype(jnp.bfloat16)
    partial_value = jnp.dot(hidden, w_down, preferred_element_type=jnp.float32).astype(jnp.bfloat16)
    returned = lax.all_to_all(
        partial_value.reshape(block.shape), "ep", split_axis=0, concat_axis=0, tiled=True
    )
    summed = jnp.sum(returned.reshape(experts, PIECES, capacity, width).astype(jnp.float32), axis=1)
    summed = summed.reshape(experts * capacity, width)
    raised = jnp.exp(route_logits)
    weights = raised / jnp.sum(raised, axis=-1, keepdims=True)
    mix_table = jnp.einsum("ske,sk->se", table, weights)
    moe = jnp.dot(mix_table, summed)
    result = (x_second + rms_scale(moe) * gain_ffn_post).astype(jnp.bfloat16)
    return (result, new_state)


def solution(mesh):
    in_specs = (
        P("ep", None),
        P(),
        P(None, "ep"),
        P(None, "ep"),
        P(None, "ep"),
        P(None, "ep"),
        P(),
        P(),
        P(),
        P(),
        P(),
        P(),
        P(),
        P("ep", None, None, None),
        P(),
        P("ep", None),
        P("ep", None),
        P(None, "ep"),
        P(None, "ep"),
        P("ep", None),
        P(),
    )
    out_specs = (P("ep", None), P("ep", None, None, None))
    return jax.shard_map(shards, mesh=mesh, in_specs=in_specs, out_specs=out_specs, check_vma=False)
```

profile of v0, /device:TPU:1, one launch (start us, length us, event | category | flops | bytes accessed | tf_op | source)
XLA Modules:
  0.0 186.9 jit_solution(18092461676442256661)
XLA Ops:
  7.2 1.0 fusion.38
  8.3 1.5 fusion.40
  9.7 0.7 neg.38
  10.4 0.8 copy.47
  11.2 0.1 eq.29
  11.4 0.2 select_reduce_fusion
  11.6 0.1 reshape.109
  11.6 1.0 fusion.12
  12.6 1.0 fusion.57
  13.6 1.0 pad_maximum_fusion
  14.6 67.3 %all-gather.2.cloned.1.call-done = bf16[1024,2048]{1,0:T(8,128)(2,1)} async-done(((bf16[8,2048]{1,0:T(8,128)(2,1)}), bf16[1024,2048]{1,0:T(8,128)(2,1)}) %all-gather.2.cloned.1.call-update) | async-done | bytes 4194320 | tf_op jit(solution)/shard_map/all_gather | solution.py:87
  81.9 3.6 %fusion.65 = f32[1024,64]{0,1:S(1)} fusion(bf16[1024,2048]{1,0:T(8,128)(2,1)} %all-gather.2.cloned.1.call-done, bf16[2048,64]{0,1:T(8,128)(2,1)S(1)} %bitcast.103), kind=kOutput, calls=%fused_computation.116 | convolution fusion | flops 268435456 | bytes 4718592
  85.5 0.7 copy.41
  86.2 1.5 reshape.127
  87.7 5.5 %all-to-all-start = ((bf16[128,2,256]{2,1,0:T(2,128)(2,1)}), bf16[128,2,256]{2,1,0:T(2,128)(2,1)S(1)}, u32[]{:S(2)}, u32[]{:S(2)}) async-start(bf16[128,2,256]{2,1,0:T(2,128)(2,1)} %reshape.127), calls=%async_computation | async-start | bytes 262144 | tf_op jit(solution)/shard_map/all_to_all | solution.py:91
  93.3 0.1 copy.49
  93.4 0.1 convert_reduce_fusion.1
  93.5 9.8 %all-to-all-done = bf16[128,2,256]{2,1,0:T(2,128)(2,1)S(1)} async-done(((bf16[128,2,256]{2,1,0:T(2,128)(2,1)}), bf16[128,2,256]{2,1,0:T(2,128)(2,1)S(1)}, u32[]{:S(2)}, u32[]{:S(2)}) %all-to-all-start) | async-done | bytes 131104 | tf_op jit(solution)/shard_map/all_to_all | solution.py:91
  103.3 0.7 reshape.128
  104.0 0.1 copy.70
  104.1 0.2 copy.43
  104.3 1.8 all_to_all.22
  106.1 0.1 multiply_reduce_fusion.4
  106.3 0.1 multiply_bitcast_fusion
  106.4 3.6 %fusion = f32[8,16,1,128]{3,2,1,0:T(1,128)S(1)} fusion(bf16[8,16,128,128]{3,2,1,0:T(8,128)(2,1)} %param.34, f32[8,16]{1,0:T(8,128)S(1)} %fusion.57, bf16[8,16,128,1]{2,0,1,3:T(8,128)(2,1)S(1)} %get-tuple-element.5), kind=kOutput, calls=%fused_computation.2 | convolution fusion | flops 8388608 | bytes 4293120 | tf_op jit(solution)/shard_map/rhk,rhkv->rhv/dot_general | solution.py:49
  110.0 0.1 broadcast_multiply_fusion
  110.2 3.8 %fusion.2 = f32[8,16,1,128]{3,2,1,0:T(1,128)S(1)} fusion(bf16[8,16,128,128]{3,2,1,0:T(8,128)(2,1)S(1)} %copy-done.1, f32[8,16,128]{2,1,0:T(8,128)S(1)} %copy.46, f32[8,16,128]{2,1,0:T(8,128)S(1)} %copy.44, f32[8,16]{1,0:T(8,128)S(1)} %fusion.57, bf16[8,16,128,1]{2,0,1,3:T(8,128)(2,1)S(1)} %get-tuple-element.4), kind=kOutput, calls=%fused_computation.4 | convolution fusion | flops 12582912 | bytes 4424192 | tf_op jit(solution)/shard_map/rhk,rhkv->rhv/dot_general | solution.py:51
  114.0 0.1 fusion.41
  114.1 4.7 %multiply_reduce_fusion.2 = (f32[8]{0:T(128)S(1)}, f32[8,2048]{1,0:T(8,128)S(1)}) fusion(bf16[2048,2048]{1,0:T(8,128)(2,1)} %param.32, f32[8,16,1,128]{3,2,1,0:T(1,128)S(1)} %fusion.2, bf16[8,4,2048]{2,0,1:T(8,128)(2,1)S(1)} %all_to_all.22, f32[128]{0:T(128)S(1)} %copy-done.7, f32[8,16]{0,1:T(8,128)S(1)} %add_rsqrt_fusion), kind=kOutput, calls=%fused_computation.73 | convolution fusion | flops 67289080 | bytes 8561184 | tf_op jit(solution)/shard_map/dot_general | solution.py:106
  118.9 0.2 multiply_reduce_fusion.1
  119.1 0.3 convolution_convert_fusion.1
  119.4 0.2 broadcast_in_dim.4
  119.6 1.6 broadcast_in_dim.5
  121.2 4.2 %all-to-all-start.1 = ((bf16[128,2,2048]{2,1,0:T(2,128)(2,1)}), bf16[128,2,2048]{2,1,0:T(2,128)(2,1)S(1)}, u32[]{:S(2)}, u32[]{:S(2)}) async-start(bf16[128,2,2048]{2,1,0:T(2,128)(2,1)} %bitcast.25), calls=%async_computation.1 | async-start | bytes 2097152 | tf_op jit(solution)/shard_map/all_to_all | solution.py:119
  125.5 19.2 %all-to-all-done.1 = bf16[128,2,2048]{2,1,0:T(2,128)(2,1)S(1)} async-done(((bf16[128,2,2048]{2,1,0:T(2,128)(2,1)}), bf16[128,2,2048]{2,1,0:T(2,128)(2,1)S(1)}, u32[]{:S(2)}, u32[]{:S(2)}) %all-to-all-start.1) | async-done | bytes 1048608 | tf_op jit(solution)/shard_map/all_to_all | solution.py:119
  144.7 1.2 reshape.111
  145.9 3.4 %convolution_minimum_fusion = f32[256,512]{1,0:T(8,128)} fusion(bf16[256,2048]{1,0:T(8,128)(2,1)} %reshape.111, bf16[2048,512]{1,0:T(8,128)(2,1)} %param.38), kind=kOutput, calls=%fused_computation.13 | convolution fusion | flops 537001984 | bytes 3670016 | tf_op jit(solution)/shard_map/dot_general | solution.py:122
  149.3 3.4 %convolution_convert_fusion = bf16[256,2048]{1,0:T(8,128)(2,1)S(1)} fusion(bf16[512,2048]{1,0:T(8,128)(2,1)S(1)} %copy-done, bf16[256,2048]{1,0:T(8,128)(2,1)} %reshape.111, bf16[2048,512]{1,0:T(8,128)(2,1)} %param.39, f32[256,512]{1,0:T(8,128)} %convolution_minimum_fusion), kind=kOutput, calls=%fused_computation.9 | convolution fusion | flops 1075445760 | bytes 6815744 | tf_op jit(solution)/shard_map/dot_general | solution.py:125
  152.6 1.5 reshape.112
  154.2 4.4 %all-to-all-start.2 = ((bf16[128,2,2048]{2,1,0:T(2,128)(2,1)}), bf16[128,2,2048]{2,1,0:T(2,128)(2,1)S(1)}, u32[]{:S(2)}, u32[]{:S(2)}) async-start(bf16[128,2,2048]{2,1,0:T(2,128)(2,1)} %reshape.112), calls=%async_computation.2 | async-start | bytes 2097152 | tf_op jit(solution)/shard_map/all_to_all | solution.py:126
  158.6 0.1 copy.55
  158.8 0.1 fusion.54
  158.9 6.0 %fusion.1 = bf16[8,16,128,128]{3,2,1,0:T(8,128)(2,1)} fusion(bf16[8,16,128,128]{3,2,1,0:T(8,128)(2,1)} %param.34, f32[8,16,128]{2,1,0:T(8,128)S(1)} %copy.46, f32[8,16,128]{2,1,0:T(8,128)S(1)} %copy.44, f32[8,16]{1,0:T(8,128)S(1)} %fusion.57), kind=kLoop, calls=%fused_computation.3 | loop fusion | flops 10485760 | bytes 8520192 | tf_op jit(solution)/shard_map/convert_element_type | solution.py:54
  164.9 13.0 %all-to-all-done.2 = bf16[128,2,2048]{2,1,0:T(2,128)(2,1)S(1)} async-done(((bf16[128,2,2048]{2,1,0:T(2,128)(2,1)}), bf16[128,2,2048]{2,1,0:T(2,128)(2,1)S(1)}, u32[]{:S(2)}, u32[]{:S(2)}) %all-to-all-start.2) | async-done | bytes 1048608 | tf_op jit(solution)/shard_map/all_to_all | solution.py:126
  177.9 1.0 convert_reduce_fusion
  179.0 0.1 reshape.113
  179.1 0.3 multiply_reduce_fusion
  179.4 0.7 add_convert_fusion
  (34 shorter events, 0.5 us)
Async XLA Ops:
  7.2 142.1 %copy-start = (bf16[512,2048]{1,0:T(8,128)(2,1)S(1)}, bf16[512,2048]{1,0:T(8,128)(2,1)}, u32[]{:S(2)}) copy-start(bf16[512,2048]{1,0:T(8,128)(2,1)} %param.40) | copy-start | bytes 6291460
  7.2 74.7 %all-gather.2.cloned.1.call-start = ((), (), s32[]{:S(2)}) async-start(), calls=%async_computation.3 | async-start | bytes 4227072 | tf_op jit(solution)/shard_map/all_gather | solution.py:87
  87.7 15.5 %all-to-all-start = ((bf16[128,2,256]{2,1,0:T(2,128)(2,1)}), bf16[128,2,256]{2,1,0:T(2,128)(2,1)S(1)}, u32[]{:S(2)}, u32[]{:S(2)}) async-start(bf16[128,2,256]{2,1,0:T(2,128)(2,1)} %reshape.127), calls=%async_computation | async-start | bytes 262144 | tf_op jit(solution)/shard_map/all_to_all | solution.py:91
  106.1 4.0 %copy-start.1 = (bf16[8,16,128,128]{3,2,1,0:T(8,128)(2,1)S(1)}, bf16[8,16,128,128]{3,2,1,0:T(8,128)(2,1)}, u32[]{:S(2)}) copy-start(bf16[8,16,128,128]{3,2,1,0:T(8,128)(2,1)} %param.34) | copy-start | bytes 12582916
  110.2 3.9 %copy-start.7 = (f32[128]{0:T(128)S(1)}, f32[128]{0:T(128)}, u32[]{:S(2)}) copy-start(f32[128]{0:T(128)} %param.31) | copy-start | bytes 1540
  114.1 4.8 %copy-start.2 = (bf16[8,2048]{1,0:T(8,128)(2,1)S(1)}, bf16[8,2048]{1,0:T(8,128)(2,1)}, u32[]{:S(2)}) copy-start(bf16[8,2048]{1,0:T(8,128)(2,1)} %param.21) | copy-start | bytes 98308
  114.1 4.8 %copy-start.3 = (f32[2048]{0:T(1024)S(1)}, f32[2048]{0:T(1024)}, u32[]{:S(2)}) copy-start(f32[2048]{0:T(1024)} %param.33) | copy-start | bytes 24580
  114.1 5.0 %copy-start.4 = (f32[2048]{0:T(1024)S(1)}, f32[2048]{0:T(1024)}, u32[]{:S(2)}) copy-start(f32[2048]{0:T(1024)} %param.35) | copy-start | bytes 24580
  118.9 6.6 %copy-start.5 = (f32[8,4]{0,1:T(4,128)S(1)}, f32[8,4]{0,1:T(4,128)}, u32[]{:S(2)}) copy-start(f32[8,4]{0,1:T(4,128)} %param.37) | copy-start | bytes 388
  121.2 23.4 %all-to-all-start.1 = ((bf16[128,2,2048]{2,1,0:T(2,128)(2,1)}), bf16[128,2,2048]{2,1,0:T(2,128)(2,1)S(1)}, u32[]{:S(2)}, u32[]{:S(2)}) async-start(bf16[128,2,2048]{2,1,0:T(2,128)(2,1)} %bitcast.25), calls=%async_computation.1 | async-start | bytes 2097152 | tf_op jit(solution)/shard_map/all_to_all | solution.py:119
  154.2 23.8 %all-to-all-start.2 = ((bf16[128,2,2048]{2,1,0:T(2,128)(2,1)}), bf16[128,2,2048]{2,1,0:T(2,128)(2,1)S(1)}, u32[]{:S(2)}, u32[]{:S(2)}) async-start(bf16[128,2,2048]{2,1,0:T(2,128)(2,1)} %reshape.112), calls=%async_computation.2 | async-start | bytes 2097152 | tf_op jit(solution)/shard_map/all_to_all | solution.py:126
  158.9 20.4 %copy-start.6 = (f32[2048]{0:T(1024)S(1)}, f32[2048]{0:T(1024)}, u32[]{:S(2)}) copy-start(f32[2048]{0:T(1024)} %param.41) | copy-start | bytes 24580
Sparse Core Ops, SparseCore 0:
  11.7 70.1 all-gather.1
where the time goes:
time: 188 us; the launch traced here: 187 us
  waiting for transfers between devices  109 us (58%)
  matrix products  25.2 us (13%)
  between operations  14.3 us (8%)
  starting transfers between devices  14.2 us (8%)
  other arithmetic  13 us (7%)
  local copies, waits for them, and re-layouts  10.9 us (6%)
    all_gather x1, waiting for transfers between devices, shards(): lax.all_gather(normed, 'ep', axis=0, tiled=True)  67.3 us
    all_to_all x1, waiting for transfers between devices, shards(): block = lax.all_to_all(sent, 'ep', split_axis=0, concat_axis=0, tiled=True)  19.2 us
    all_to_all x1, waiting for transfers between devices, shards(): lax.all_to_all(partial_value.reshape(block.shape), 'ep', split_axis=0, co...  13 us
    all_to_all x1, waiting for transfers between devices, shards(): lax.all_to_all(columns, 'ep', split_axis=0, concat_axis=2, tiled=True)  9.77 us
    convert_element_type x1, other arithmetic, delta_step(): return (gated.astype(jnp.bfloat16), held.astype(jnp.bfloat16))  5.96 us
    all_to_all x1, starting transfers between devices, shards(): lax.all_to_all(columns, 'ep', split_axis=0, concat_axis=2, tiled=True)  5.51 us
    dot_general x1, matrix products, shards(): branch = jnp.dot(mixed, w_out, preferred_element_type=jnp.float32)  4.73 us
    all_to_all x1, starting transfers between devices, shards(): lax.all_to_all(partial_value.reshape(block.shape), 'ep', split_axis=0, co...  4.43 us
  transfers between devices with their start and end apart: 4, of which 4 were waited for; matrix products, arithmetic and copies ran while one was open for 6% of the time, Pallas kernels for 0%

commit v1 on v0

--- a/solution.py
+++ b/solution.py
@@ -84,7 +84,9 @@
     stacked = jnp.stack([w_query, w_key, w_value, w_outgate])
     columns = jnp.einsum(
         "td,rdc->trc",
-        lax.all_gather(normed, "ep", axis=0, tiled=True),
+        jnp.concatenate(
+            lax.all_to_all(jnp.stack([normed] * lax.axis_size("ep")), "ep", 0, 0), axis=0
+        ),
         stacked,
         preferred_element_type=jnp.float32,
     ).astype(jnp.bfloat16)

time: 188 us -> 167 us (0.89)
  waiting for transfers between devices: 109 us -> 93.7 us
  between operations: 14.3 us -> 1.07 us
  starting transfers between devices: 14.2 us -> 25 us
  other arithmetic: 13 us -> 10.8 us
  local copies, waits for them, and re-layouts: 10.9 us -> 12.8 us
    all_gather x1 -> x0, waiting for transfers between devices: 67.3 us -> none  [shards(): lax.all_gather(normed, 'ep', axis=0, tiled=True)]
    all_to_all x0 -> x1, waiting for transfers between devices: none -> 51.6 us  [shards(): lax.all_to_all(jnp.stack([normed] * lax.axis_size('ep')), 'ep', 0, 0)]
    all_to_all x0 -> x1, starting transfers between devices: none -> 12 us  [shards(): lax.all_to_all(jnp.stack([normed] * lax.axis_size('ep')), 'ep', 0, 0)]
    another operation x0 -> x1, local copies, waits for them, and re-layouts: none -> 2.54 us  [shards(): jnp.stack([normed] * lax.axis_size('ep'))]
  transfers between devices with their start and end apart: 4 -> 4, of which waited for: 4 -> 4; matrix products, arithmetic and copies ran while one was open for 6% -> 4% of each run, Pallas kernels for 0% -> 0%
where the time goes in v1:
time: 167 us
  waiting for transfers between devices  93.7 us (56%)
  starting transfers between devices  25 us (15%)
  matrix products  23.4 us (14%)
  local copies, waits for them, and re-layouts  12.8 us (8%)
  other arithmetic  10.8 us (6%)
    all_to_all x1, waiting for transfers between devices, shards(): lax.all_to_all(jnp.stack([normed] * lax.axis_size('ep')), 'ep', 0, 0)  51.6 us
    all_to_all x1, waiting for transfers between devices, shards(): block = lax.all_to_all(sent, 'ep', split_axis=0, concat_axis=0, tiled=True)  19.2 us
    all_to_all x1, waiting for transfers between devices, shards(): lax.all_to_all(partial_value.reshape(block.shape), 'ep', split_axis=0, co...  13 us
    all_to_all x1, starting transfers between devices, shards(): lax.all_to_all(jnp.stack([normed] * lax.axis_size('ep')), 'ep', 0, 0)  12 us
    all_to_all x1, waiting for transfers between devices, shards(): lax.all_to_all(columns, 'ep', split_axis=0, concat_axis=2, tiled=True)  9.91 us
    convert_element_type x1, other arithmetic, delta_step(): return (gated.astype(jnp.bfloat16), held.astype(jnp.bfloat16))  5.96 us
    dot_general x1, matrix products, shards(): branch = jnp.dot(mixed, w_out, preferred_element_type=jnp.float32)  4.73 us
    all_to_all x1, starting transfers between devices, shards(): lax.all_to_all(partial_value.reshape(block.shape), 'ep', split_axis=0, co...  4.43 us
  transfers between devices with their start and end apart: 4, of which 4 were waited for; matrix products, arithmetic and copies ran while one was open for 4% of the time, Pallas kernels for 0%

profile of v1, /device:TPU:1, one launch (start us, length us, event | category | flops | bytes accessed | tf_op | source)
XLA Modules:
  0.0 166.9 jit_solution(10750980709047537673)
XLA Ops:
  0.6 1.0 fusion.40
  1.7 0.8 fusion.42
  2.5 2.5 %stack.12 = bf16[128,8,2048]{2,1,0:T(8,128)(2,1)} broadcast(bf16[8,2048]{1,0:T(8,128)(2,1)S(1)} %fusion.42), dimensions={1,2} | broadcast | bytes 4227072 | tf_op jit(solution)/shard_map/stack | solution.py:88
  5.1 12.0 %all-to-all-start = ((bf16[128,8,2048]{2,1,0:T(8,128)(2,1)}), bf16[128,8,2048]{2,1,0:T(8,128)(2,1)}, u32[]{:S(2)}, u32[]{:S(2)}) async-start(bf16[128,8,2048]{2,1,0:T(8,128)(2,1)} %stack.12), calls=%async_computation | async-start | bytes 8388608 | tf_op jit(solution)/shard_map/all_to_all | solution.py:88
  17.1 0.1 copy.47
  17.2 0.1 eq.29
  17.4 0.2 select_reduce_fusion
  17.6 0.1 reshape.115
  17.7 0.1 fusion.14
  17.9 0.1 fusion.59
  18.1 51.6 %all-to-all-done = bf16[128,8,2048]{2,1,0:T(8,128)(2,1)} async-done(((bf16[128,8,2048]{2,1,0:T(8,128)(2,1)}), bf16[128,8,2048]{2,1,0:T(8,128)(2,1)}, u32[]{:S(2)}, u32[]{:S(2)}) %all-to-all-start) | async-done | bytes 4194336 | tf_op jit(solution)/shard_map/all_to_all | solution.py:88
  69.7 3.6 %fusion.3 = f32[1024,64]{0,1:S(1)} fusion(bf16[2048,64]{0,1:T(8,128)(2,1)S(1)} %bitcast.105, bf16[128,8,2048]{2,1,0:T(8,128)(2,1)} %all-to-all-done), kind=kOutput, calls=%fused_computation.5 | convolution fusion | flops 268435456 | bytes 4718592
  73.3 0.7 copy.41
  74.0 1.5 reshape.133
  75.5 4.4 %all-to-all-start.1 = ((bf16[128,2,256]{2,1,0:T(2,128)(2,1)}), bf16[128,2,256]{2,1,0:T(2,128)(2,1)S(1)}, u32[]{:S(2)}, u32[]{:S(2)}) async-start(bf16[128,2,256]{2,1,0:T(2,128)(2,1)} %reshape.133), calls=%async_computation.1 | async-start | bytes 262144 | tf_op jit(solution)/shard_map/all_to_all | solution.py:93
  80.0 0.1 copy.49
  80.1 0.1 convert_reduce_fusion.1
  80.1 9.9 %all-to-all-done.1 = bf16[128,2,256]{2,1,0:T(2,128)(2,1)S(1)} async-done(((bf16[128,2,256]{2,1,0:T(2,128)(2,1)}), bf16[128,2,256]{2,1,0:T(2,128)(2,1)S(1)}, u32[]{:S(2)}, u32[]{:S(2)}) %all-to-all-start.1) | async-done | bytes 131104 | tf_op jit(solution)/shard_map/all_to_all | solution.py:93
  90.1 0.7 reshape.134
  90.7 0.1 copy.70
  90.9 0.2 copy.43
  91.1 1.8 %all_to_all.26 = bf16[8,4,2048]{2,0,1:T(8,128)(2,1)S(1)} reshape(bf16[8,4,128,16]{3,2,0,1:T(8,128)(2,1)S(1)} %copy.43) | data formatting | bytes 262144 | tf_op jit(solution)/shard_map/all_to_all | solution.py:93
  92.9 0.1 multiply_reduce_fusion.4
  93.1 0.1 multiply_bitcast_fusion
  93.2 3.6 %fusion = f32[8,16,1,128]{3,2,1,0:T(1,128)S(1)} fusion(bf16[8,16,128,128]{3,2,1,0:T(8,128)(2,1)} %param.34, f32[8,16]{1,0:T(8,128)S(1)} %fusion.59, bf16[8,16,128,1]{2,0,1,3:T(8,128)(2,1)S(1)} %get-tuple-element.5), kind=kOutput, calls=%fused_computation.2 | convolution fusion | flops 8388608 | bytes 4293120 | tf_op jit(solution)/shard_map/rhk,rhkv->rhv/dot_general | solution.py:49
  96.8 0.1 broadcast_multiply_fusion
  97.0 3.8 %fusion.2 = f32[8,16,1,128]{3,2,1,0:T(1,128)S(1)} fusion(bf16[8,16,128,128]{3,2,1,0:T(8,128)(2,1)S(1)} %copy-done.1, f32[8,16,128]{2,1,0:T(8,128)S(1)} %copy.46, f32[8,16,128]{2,1,0:T(8,128)S(1)} %copy.44, f32[8,16]{1,0:T(8,128)S(1)} %fusion.59, bf16[8,16,128,1]{2,0,1,3:T(8,128)(2,1)S(1)} %get-tuple-element.4), kind=kOutput, calls=%fused_computation.4 | convolution fusion | flops 12582912 | bytes 4424192 | tf_op jit(solution)/shard_map/rhk,rhkv->rhv/dot_general | solution.py:51
  100.8 0.1 fusion.43
  100.9 4.7 %multiply_reduce_fusion.2 = (f32[8]{0:T(128)S(1)}, f32[8,2048]{1,0:T(8,128)S(1)}) fusion(bf16[2048,2048]{1,0:T(8,128)(2,1)} %param.32, f32[8,16,1,128]{3,2,1,0:T(1,128)S(1)} %fusion.2, bf16[8,4,2048]{2,0,1:T(8,128)(2,1)S(1)} %all_to_all.26, f32[128]{0:T(128)S(1)} %copy-done.15, f32[8,16]{0,1:T(8,128)S(1)} %add_rsqrt_fusion), kind=kOutput, calls=%fused_computation.75 | convolution fusion | flops 67289080 | bytes 8561184 | tf_op jit(solution)/shard_map/dot_general | solution.py:108
  105.7 0.2 multiply_reduce_fusion.1
  105.9 0.3 convolution_convert_fusion.1
  106.2 0.2 broadcast_in_dim.4
  106.4 1.6 broadcast_in_dim.5
  108.0 4.2 %all-to-all-start.2 = ((bf16[128,2,2048]{2,1,0:T(2,128)(2,1)}), bf16[128,2,2048]{2,1,0:T(2,128)(2,1)S(1)}, u32[]{:S(2)}, u32[]{:S(2)}) async-start(bf16[128,2,2048]{2,1,0:T(2,128)(2,1)} %bitcast.26), calls=%async_computation.2 | async-start | bytes 2097152 | tf_op jit(solution)/shard_map/all_to_all | solution.py:121
  112.3 19.2 %all-to-all-done.2 = bf16[128,2,2048]{2,1,0:T(2,128)(2,1)S(1)} async-done(((bf16[128,2,2048]{2,1,0:T(2,128)(2,1)}), bf16[128,2,2048]{2,1,0:T(2,128)(2,1)S(1)}, u32[]{:S(2)}, u32[]{:S(2)}) %all-to-all-start.2) | async-done | bytes 1048608 | tf_op jit(solution)/shard_map/all_to_all | solution.py:121
  131.5 1.2 reshape.117
  132.7 3.4 %convolution_minimum_fusion = f32[256,512]{1,0:T(8,128)} fusion(bf16[256,2048]{1,0:T(8,128)(2,1)} %reshape.117, bf16[2048,512]{1,0:T(8,128)(2,1)} %param.38), kind=kOutput, calls=%fused_computation.15 | convolution fusion | flops 537001984 | bytes 3670016 | tf_op jit(solution)/shard_map/dot_general | solution.py:124
  136.1 3.4 %convolution_convert_fusion = bf16[256,2048]{1,0:T(8,128)(2,1)S(1)} fusion(bf16[512,2048]{1,0:T(8,128)(2,1)S(1)} %copy-done, bf16[256,2048]{1,0:T(8,128)(2,1)} %reshape.117, bf16[2048,512]{1,0:T(8,128)(2,1)} %param.39, f32[256,512]{1,0:T(8,128)} %convolution_minimum_fusion), kind=kOutput, calls=%fused_computation.11 | convolution fusion | flops 1075445760 | bytes 6815744 | tf_op jit(solution)/shard_map/dot_general | solution.py:127
  139.4 1.5 reshape.118
  141.0 4.4 %all-to-all-start.3 = ((bf16[128,2,2048]{2,1,0:T(2,128)(2,1)}), bf16[128,2,2048]{2,1,0:T(2,128)(2,1)S(1)}, u32[]{:S(2)}, u32[]{:S(2)}) async-start(bf16[128,2,2048]{2,1,0:T(2,128)(2,1)} %reshape.118), calls=%async_computation.3 | async-start | bytes 2097152 | tf_op jit(solution)/shard_map/all_to_all | solution.py:128
  145.4 0.1 copy.55
  145.6 0.1 fusion.56
  145.7 6.0 %fusion.1 = bf16[8,16,128,128]{3,2,1,0:T(8,128)(2,1)} fusion(bf16[8,16,128,128]{3,2,1,0:T(8,128)(2,1)} %param.34, f32[8,16,128]{2,1,0:T(8,128)S(1)} %copy.46, f32[8,16,128]{2,1,0:T(8,128)S(1)} %copy.44, f32[8,16]{1,0:T(8,128)S(1)} %fusion.59), kind=kLoop, calls=%fused_computation.3 | loop fusion | flops 10485760 | bytes 8520192 | tf_op jit(solution)/shard_map/convert_element_type | solution.py:54
  151.7 13.0 %all-to-all-done.3 = bf16[128,2,2048]{2,1,0:T(2,128)(2,1)S(1)} async-done(((bf16[128,2,2048]{2,1,0:T(2,128)(2,1)}), bf16[128,2,2048]{2,1,0:T(2,128)(2,1)S(1)}, u32[]{:S(2)}, u32[]{:S(2)}) %all-to-all-start.3) | async-done | bytes 1048608 | tf_op jit(solution)/shard_map/all_to_all | solution.py:128
  164.7 1.0 convert_reduce_fusion
  165.8 0.1 reshape.119
  165.9 0.3 multiply_reduce_fusion
  166.2 0.7 add_convert_fusion
  (52 shorter events, 0.5 us)
Async XLA Ops:
  0.6 135.4 %copy-start = (bf16[512,2048]{1,0:T(8,128)(2,1)S(1)}, bf16[512,2048]{1,0:T(8,128)(2,1)}, u32[]{:S(2)}) copy-start(bf16[512,2048]{1,0:T(8,128)(2,1)} %param.40) | copy-start | bytes 6291460
  5.1 12.0 %copy-start.16 = (f32[16]{0:T(128)S(1)}, f32[16]{0:T(128)}, u32[]{:S(2)}) copy-start(f32[16]{0:T(128)} %param.29) | copy-start | bytes 196
  5.1 12.1 %copy-start.13 = (s32[8,4]{0,1:T(4,128)S(1)}, s32[8,4]{0,1:T(4,128)}, u32[]{:S(2)}) copy-start(s32[8,4]{0,1:T(4,128)} %param.36) | copy-start | bytes 388
  5.1 12.6 %copy-start.4 = (bf16[2048,16]{0,1:T(8,128)(2,1)S(1)}, bf16[2048,16]{0,1:T(8,128)(2,1)}, u32[]{:S(2)}) copy-start(bf16[2048,16]{0,1:T(8,128)(2,1)} %param.28) | copy-start | bytes 196612
  5.1 12.8 %copy-start.5 = (bf16[2048,16]{0,1:T(8,128)(2,1)S(1)}, bf16[2048,16]{0,1:T(8,128)(2,1)}, u32[]{:S(2)}) copy-start(bf16[2048,16]{0,1:T(8,128)(2,1)} %param.27) | copy-start | bytes 196612
  5.1 12.8 %copy-start.14 = (f32[16]{0:T(128)S(1)}, f32[16]{0:T(128)}, u32[]{:S(2)}) copy-start(f32[16]{0:T(128)} %param.30) | copy-start | bytes 196
  5.1 12.9 %copy-start.6 = (bf16[2048,16]{0,1:T(8,128)(2,1)S(1)}, bf16[2048,16]{0,1:T(8,128)(2,1)}, u32[]{:S(2)}) copy-start(bf16[2048,16]{0,1:T(8,128)(2,1)} %param.26) | copy-start | bytes 196612
  5.1 12.9 %copy-start.7 = (bf16[2048,16]{0,1:T(8,128)(2,1)S(1)}, bf16[2048,16]{0,1:T(8,128)(2,1)}, u32[]{:S(2)}) copy-start(bf16[2048,16]{0,1:T(8,128)(2,1)} %param.25) | copy-start | bytes 196612
  5.1 12.9 %copy-start.8 = (bf16[2048,16]{0,1:T(8,128)(2,1)S(1)}, bf16[2048,16]{0,1:T(8,128)(2,1)}, u32[]{:S(2)}) copy-start(bf16[2048,16]{0,1:T(8,128)(2,1)} %param.24) | copy-start | bytes 196612
  5.1 12.9 %copy-start.9 = (bf16[2048,16]{0,1:T(8,128)(2,1)S(1)}, bf16[2048,16]{0,1:T(8,128)(2,1)}, u32[]{:S(2)}) copy-start(bf16[2048,16]{0,1:T(8,128)(2,1)} %param.23) | copy-start | bytes 196612
  5.1 64.5 %all-to-all-start = ((bf16[128,8,2048]{2,1,0:T(8,128)(2,1)}), bf16[128,8,2048]{2,1,0:T(8,128)(2,1)}, u32[]{:S(2)}, u32[]{:S(2)}) async-start(bf16[128,8,2048]{2,1,0:T(8,128)(2,1)} %stack.12), calls=%async_computation | async-start | bytes 8388608 | tf_op jit(solution)/shard_map/all_to_all | solution.py:88
  75.5 14.5 %all-to-all-start.1 = ((bf16[128,2,256]{2,1,0:T(2,128)(2,1)}), bf16[128,2,256]{2,1,0:T(2,128)(2,1)S(1)}, u32[]{:S(2)}, u32[]{:S(2)}) async-start(bf16[128,2,256]{2,1,0:T(2,128)(2,1)} %reshape.133), calls=%async_computation.1 | async-start | bytes 262144 | tf_op jit(solution)/shard_map/all_to_all | solution.py:93
  92.9 4.0 %copy-start.1 = (bf16[8,16,128,128]{3,2,1,0:T(8,128)(2,1)S(1)}, bf16[8,16,128,128]{3,2,1,0:T(8,128)(2,1)}, u32[]{:S(2)}) copy-start(bf16[8,16,128,128]{3,2,1,0:T(8,128)(2,1)} %param.34) | copy-start | bytes 12582916
  96.9 3.9 %copy-start.15 = (f32[128]{0:T(128)S(1)}, f32[128]{0:T(128)}, u32[]{:S(2)}) copy-start(f32[128]{0:T(128)} %param.31) | copy-start | bytes 1540
  100.9 4.8 %copy-start.2 = (bf16[8,2048]{1,0:T(8,128)(2,1)S(1)}, bf16[8,2048]{1,0:T(8,128)(2,1)}, u32[]{:S(2)}) copy-start(bf16[8,2048]{1,0:T(8,128)(2,1)} %param.21) | copy-start | bytes 98308
  100.9 4.8 %copy-start.3 = (f32[2048]{0:T(1024)S(1)}, f32[2048]{0:T(1024)}, u32[]{:S(2)}) copy-start(f32[2048]{0:T(1024)} %param.33) | copy-start | bytes 24580
  100.9 5.0 %copy-start.10 = (f32[2048]{0:T(1024)S(1)}, f32[2048]{0:T(1024)}, u32[]{:S(2)}) copy-start(f32[2048]{0:T(1024)} %param.35) | copy-start | bytes 24580
  105.7 6.6 %copy-start.11 = (f32[8,4]{0,1:T(4,128)S(1)}, f32[8,4]{0,1:T(4,128)}, u32[]{:S(2)}) copy-start(f32[8,4]{0,1:T(4,128)} %param.37) | copy-start | bytes 388
  108.0 23.4 %all-to-all-start.2 = ((bf16[128,2,2048]{2,1,0:T(2,128)(2,1)}), bf16[128,2,2048]{2,1,0:T(2,128)(2,1)S(1)}, u32[]{:S(2)}, u32[]{:S(2)}) async-start(bf16[128,2,2048]{2,1,0:T(2,128)(2,1)} %bitcast.26), calls=%async_computation.2 | async-start | bytes 2097152 | tf_op jit(solution)/shard_map/all_to_all | solution.py:121
  141.0 23.8 %all-to-all-start.3 = ((bf16[128,2,2048]{2,1,0:T(2,128)(2,1)}), bf16[128,2,2048]{2,1,0:T(2,128)(2,1)S(1)}, u32[]{:S(2)}, u32[]{:S(2)}) async-start(bf16[128,2,2048]{2,1,0:T(2,128)(2,1)} %reshape.118), calls=%async_computation.3 | async-start | bytes 2097152 | tf_op jit(solution)/shard_map/all_to_all | solution.py:128
  145.7 20.4 %copy-start.12 = (f32[2048]{0:T(1024)S(1)}, f32[2048]{0:T(1024)}, u32[]{:S(2)}) copy-start(f32[2048]{0:T(1024)} %param.41) | copy-start | bytes 24580
